TPU v7x, 32 devices: a whole 2x2x4 slice. The times are simulated.
32 devices in a mesh: kv: 16 (over z, y, x), tp: 2 (over core).
Axes of the slice: x: 2, y: 2, z: 4, core: 2. Of those that a mesh axis runs over, the one named last changes fastest.
Arguments:
- queries: bfloat16 [4096, 1024], P('kv', 'tp'), may hold values from -4 to 4
- keys: bfloat16 [4096, 1024], P('kv', 'tp'), may hold values from -4 to 4
- values: bfloat16 [4096, 1024], P('kv', 'tp'), may hold values from -5 to 5
- log_sums: float32 [16, 4096], P('tp', 'kv'), may hold values from 5.5 to 7
- out_grad: bfloat16 [4096, 1024], P('kv', 'tp'), may hold values from -24 to 24
- chosen: int32 [32, 8], P('kv'), may hold values from -1 to 127, as said below
- normed: bfloat16 [4096, 2048], P('kv', 'tp'), may hold values from -0.23925781 to 0.23925781
Outputs:
- query_grad: bfloat16 [4096, 1024], P('kv', 'tp')
- key_grad: bfloat16 [4096, 1024], P('kv', 'tp')
- value_grad: bfloat16 [4096, 1024], P('kv', 'tp')
- weight_grad: float32 [2048, 1024], P('kv', 'tp')
Inputs may be any that keep to these rules, and one draw needn't show every extreme that they name: `chosen`: each used entry names a key block that ends at or before its query block's start; the used entries of one list are distinct. Among the lists of the 2 query blocks of one index of kv, the key blocks of any other index of kv appear as at most one distinct block; for every index from 1 on, the first query block's list names a block of the index before, and the last index's first query block's list names a block of index 0. Blocks of the own index of kv before the query block may appear freely.
All inputs are finite; a program needn't handle non-finite values.
Results may differ from a plain program's by a relative error of at most 0.008.
Values may be sent and summed in bfloat16 or wider, within the bound.
A program may use at most 64 MiB of HBM per device.

v0:
```python
from functools import partial
import jax
import jax.numpy as jnp
from jax import lax
from jax.sharding import PartitionSpec as P

QB = 128
KB = 32


def block_grads(inputs, scaling):
    query_blk, grad_blk, sums_blk, keys_sel, vals_sel, keys_own, vals_own, eligible_blocks = inputs
    span_rows = query_blk.shape[0]
    scores = (
        jnp.einsum("qhd,skhd->hqsk", query_blk, keys_sel, preferred_element_type=jnp.float32)
        * scaling
    )
    weights = jnp.where(
        eligible_blocks[None, None, :, None], jnp.exp(scores - sums_blk[:, :, None, None]), 0.0
    )
    causal = lax.broadcasted_iota(jnp.int32, (span_rows, span_rows), 0) >= lax.broadcasted_iota(
        jnp.int32, (span_rows, span_rows), 1
    )
    own_scores = (
        jnp.einsum("qhd,khd->hqk", query_blk, keys_own, preferred_element_type=jnp.float32)
        * scaling
    )
    own_weights = jnp.where(causal[None], jnp.exp(own_scores - sums_blk[:, :, None]), 0.0)
    weights_low = weights.astype(jnp.bfloat16)
    own_low = own_weights.astype(jnp.bfloat16)
    attended = jnp.einsum(
        "hqsk,skhd->qhd", weights_low, vals_sel, preferred_element_type=jnp.float32
    )
    attended = attended + jnp.einsum(
        "hqk,khd->qhd", own_low, vals_own, preferred_element_type=jnp.float32
    )
    deltas = jnp.sum(grad_blk.astype(jnp.float32) * attended, axis=-1).T
    dots_sel = jnp.einsum("qhd,skhd->hqsk", grad_blk, vals_sel, preferred_element_type=jnp.float32)
    own_dots = jnp.einsum("qhd,khd->hqk", grad_blk, vals_own, preferred_element_type=jnp.float32)
    slopes = (weights * (dots_sel - deltas[:, :, None, None])).astype(jnp.bfloat16)
    own_slopes = (own_weights * (own_dots - deltas[:, :, None])).astype(jnp.bfloat16)
    query_part = jnp.einsum("hqsk,skhd->qhd", slopes, keys_sel, preferred_element_type=jnp.float32)
    query_part = scaling * (
        query_part
        + jnp.einsum("hqk,khd->qhd", own_slopes, keys_own, preferred_element_type=jnp.float32)
    )
    key_terms = scaling * jnp.einsum(
        "hqsk,qhd->skhd", slopes, query_blk, preferred_element_type=jnp.float32
    )
    value_terms = jnp.einsum(
        "hqsk,qhd->skhd", weights_low, grad_blk, preferred_element_type=jnp.float32
    )
    own_key_terms = scaling * jnp.einsum(
        "hqk,qhd->khd", own_slopes, query_blk, preferred_element_type=jnp.float32
    )
    own_value_terms = jnp.einsum(
        "hqk,qhd->khd", own_low, grad_blk, preferred_element_type=jnp.float32
    )
    return (query_part.astype(jnp.bfloat16), key_terms, value_terms, own_key_terms, own_value_terms)


def body(queries, keys, values, log_sums, out_grad, chosen, normed):
    devices = lax.axis_size("kv")
    myself = lax.axis_index("kv")
    rows_here, columns = queries.shape
    head_count = log_sums.shape[0]
    head_size = columns // head_count
    query_blocks = rows_here // QB
    key_blocks = rows_here // KB
    selected = chosen.shape[1]
    groups = 1
    slot_count = devices * groups
    owners = chosen // key_blocks
    offsets = chosen % key_blocks
    eligible_blocks = chosen >= 0
    remote = eligible_blocks & (owners != myself)
    slot_ids = owners * groups
    matches = remote[:, :, None] & (
        slot_ids[:, :, None] == jnp.arange(slot_count, dtype=jnp.int32)[None, None, :]
    )
    wanted = jnp.max(jnp.where(matches, offsets[:, :, None] + 1, 0), axis=(0, 1))
    requested = lax.all_to_all(
        wanted.reshape(devices, groups), "kv", split_axis=0, concat_axis=0, tiled=True
    ).reshape(-1)
    live_request = requested > 0
    picked = jnp.clip(requested - 1, 0, key_blocks - 1)
    key_table = keys.reshape(key_blocks, KB, columns)
    value_table = values.reshape(key_blocks, KB, columns)
    zero_block = jnp.zeros((), keys.dtype)
    outgoing_keys = jnp.where(live_request[:, None, None], key_table[picked], zero_block).reshape(
        devices, groups, KB, columns
    )
    outgoing_values = jnp.where(
        live_request[:, None, None], value_table[picked], zero_block
    ).reshape(devices, groups, KB, columns)
    fetched_keys, fetched_values = (
        lax.all_to_all(outgoing_keys, "kv", split_axis=0, concat_axis=0, tiled=True),
        lax.all_to_all(outgoing_values, "kv", split_axis=0, concat_axis=0, tiled=True),
    )
    all_keys = jnp.concatenate([fetched_keys.reshape(slot_count, KB, columns), key_table], axis=0)
    all_values = jnp.concatenate(
        [fetched_values.reshape(slot_count, KB, columns), value_table], axis=0
    )
    table_ids = jnp.where(remote, slot_ids, jnp.where(eligible_blocks, slot_count + offsets, 0))
    keys_sel = all_keys[table_ids].reshape(query_blocks, selected, KB, head_count, head_size)
    vals_sel = all_values[table_ids].reshape(query_blocks, selected, KB, head_count, head_size)
    block_shape = (query_blocks, QB, head_count, head_size)
    inputs = (
        queries.reshape(block_shape),
        out_grad.reshape(block_shape),
        log_sums.reshape(head_count, query_blocks, QB).transpose(1, 0, 2),
        keys_sel,
        vals_sel,
        keys.reshape(block_shape),
        values.reshape(block_shape),
        eligible_blocks,
    )
    query_part, key_terms, value_terms, own_key_terms, own_value_terms = lax.map(
        partial(block_grads, scaling=head_size ** (-0.5)), inputs
    )
    routes = (
        table_ids.reshape(-1)[:, None]
        == jnp.arange(slot_count + key_blocks, dtype=jnp.int32)[None, :]
    ) & eligible_blocks.reshape(-1)[:, None]
    stacked_terms = jnp.stack(
        [key_terms.reshape(-1, KB * columns), value_terms.reshape(-1, KB * columns)]
    )
    routed = jnp.einsum(
        "ab,xac->xbc", routes.astype(jnp.float32), stacked_terms, precision=lax.Precision.HIGHEST
    )
    back_keys = routed[0, :slot_count].reshape(devices, groups, KB, columns)
    back_values = routed[1, :slot_count].reshape(devices, groups, KB, columns)
    returned_keys, returned_values = (
        lax.all_to_all(back_keys, "kv", split_axis=0, concat_axis=0, tiled=True),
        lax.all_to_all(back_values, "kv", split_axis=0, concat_axis=0, tiled=True),
    )
    matched = (
        ((requested - 1)[:, None] == jnp.arange(key_blocks, dtype=jnp.int32)[None, :])
        & live_request[:, None]
    ).astype(jnp.float32)
    stacked_back = jnp.stack(
        [
            returned_keys.reshape(slot_count, KB * columns),
            returned_values.reshape(slot_count, KB * columns),
        ]
    )
    arrived = jnp.einsum("ab,xac->xbc", matched, stacked_back, precision=lax.Precision.HIGHEST)
    totals = arrived + routed[:, slot_count:]
    key_grad = (
        totals[0].reshape(rows_here, columns) + own_key_terms.reshape(rows_here, columns)
    ).astype(jnp.bfloat16)
    value_grad = (
        totals[1].reshape(rows_here, columns) + own_value_terms.reshape(rows_here, columns)
    ).astype(jnp.bfloat16)
    features_all = lax.all_gather(normed, "tp", axis=1, tiled=True)
    weight_grad = lax.psum_scatter(
        lax.dot_general(
            features_all, value_grad, (((0,), (0,)), ((), ())), preferred_element_type=jnp.float32
        ),
        "kv",
        scatter_dimension=0,
        tiled=True,
    )
    return (query_part.reshape(rows_here, columns), key_grad, value_grad, weight_grad)


def solution(mesh):
    in_specs = (
        P("kv", "tp"),
        P("kv", "tp"),
        P("kv", "tp"),
        P("tp", "kv"),
        P("kv", "tp"),
        P("kv", None),
        P("kv", "tp"),
    )
    out_specs = (P("kv", "tp"), P("kv", "tp"), P("kv", "tp"), P("kv", "tp"))
    return jax.shard_map(body, mesh=mesh, in_specs=in_specs, out_specs=out_specs, check_vma=False)
```

profile of v0, /device:TPU:0, one launch (start us, length us, event | category | flops | bytes accessed | tf_op | source)
XLA Modules:
  0.0 302.4 jit_solution(817550221960606764)
XLA Ops:
  8.1 15.4 %all_to_all.29 = s32[16,1,1]{2,1,0:T(1,128)S(1)} all-to-all(s32[16,1,1]{2,1,0:T(1,128)S(1)} %copy.86), channel_id=1, replica_groups=mesh['kv'=16,'tp'=2] {'kv'}, dimensions={0} | all-to-all | bytes 128 | tf_op jit(solution)/shard_map/all_to_all | solution.py:82
  24.2 1.5 gather_fusion.2
  25.7 1.5 gather_fusion
  28.6 16.8 %all_to_all.30 = bf16[16,1,32,512]{3,2,1,0:T(8,128)(2,1)S(1)} all-to-all(bf16[16,1,32,512]{3,2,1,0:T(8,128)(2,1)S(1)} %get-tuple-element.203), channel_id=1, replica_groups=mesh['kv'=16,'tp'=2] {'kv'}, dimensions={0} | all-to-all | bytes 1048576 | tf_op jit(solution)/shard_map/all_to_all | solution.py:97
  45.3 3.9 %all-to-all-start.2 = ((bf16[16,1,32,512]{3,2,1,0:T(8,128)(2,1)}), bf16[16,1,32,512]{3,2,1,0:T(8,128)(2,1)S(1)}, u32[]{:S(2)}, u32[]{:S(2)}) async-start(bf16[16,1,32,512]{3,2,1,0:T(8,128)(2,1)} %get-tuple-element.202), calls=%async_computation.2 | async-start | bytes 1048576 | tf_op jit(solution)/shard_map/all_to_all | solution.py:98
  52.0 1.3 copy.92
  55.7 2.0 copy.95
  60.0 3.3 %all-to-all-done.2 = bf16[16,1,32,512]{3,2,1,0:T(8,128)(2,1)S(1)} async-done(((bf16[16,1,32,512]{3,2,1,0:T(8,128)(2,1)}), bf16[16,1,32,512]{3,2,1,0:T(8,128)(2,1)S(1)}, u32[]{:S(2)}, u32[]{:S(2)}) %all-to-all-start.2) | async-done | bytes 524320 | tf_op jit(solution)/shard_map/all_to_all | solution.py:98
  64.5 56.6 %while.18 = (s32[]{:T(128)}, bf16[2,128,8,64]{1,3,2,0:T(8,128)(2,1)}, f32[2,8,32,8,64]{4,3,2,1,0:T(8,128)}, f32[2,8,32,8,64]{4,3,2,1,0:T(8,128)}, f32[2,128,8,64...) while((s32[]{:T(128)}, ...), condition=%wide.region_3.4_spmd, body=%wide.region_1.3_spmd.sunk | while | flops 306330624 | bytes 43585888 | solution.py:118
  70.4 1.9 fusion.160
  74.5 1.9 copy_dynamic-update-slice_fusion.3
  78.4 7.1 %dynamic_update_slice.27 = f32[2,128,8,64]{1,0,3,2:T(2,128)} dynamic-update-slice(f32[2,128,8,64]{1,0,3,2:T(2,128)} %get-tuple-element.313, f32[1,128,8,64]{1,0,3,2:T(1,128)S(1)} %bitcast.262, s32[]{:T(128)S(6)} %copy.169, s32[]{:T(128)} %constant.73.clone.1..sunk, s32[]{:T(128)} %constant.73.clone.1..sunk, s32[]{:T(128)} %constant.73.clone.1..sunk) | dynamic-update-slice | bytes 524292 | tf_op jit(solution)/shard_map/while/body/jit(dynamic_update_index_in_dim)/dynamic_update_slice | solution.py:118
  85.7 7.1 %dynamic_update_slice.28 = f32[2,128,8,64]{1,0,3,2:T(2,128)} dynamic-update-slice(f32[2,128,8,64]{1,0,3,2:T(2,128)} %get-tuple-element.314, f32[1,128,8,64]{1,0,3,2:T(1,128)S(1)} %bitcast.261, s32[]{:T(128)S(6)} %copy.169, s32[]{:T(128)} %constant.73.clone.1..sunk, s32[]{:T(128)} %constant.73.clone.1..sunk, s32[]{:T(128)} %constant.73.clone.1..sunk) | dynamic-update-slice | bytes 524292 | tf_op jit(solution)/shard_map/while/body/jit(dynamic_update_index_in_dim)/dynamic_update_slice | solution.py:118
  98.7 1.9 fusion.160
  102.8 1.9 copy_dynamic-update-slice_fusion.3
  106.7 7.1 %dynamic_update_slice.27 = f32[2,128,8,64]{1,0,3,2:T(2,128)} dynamic-update-slice(f32[2,128,8,64]{1,0,3,2:T(2,128)} %get-tuple-element.313, f32[1,128,8,64]{1,0,3,2:T(1,128)S(1)} %bitcast.262, s32[]{:T(128)S(6)} %copy.169, s32[]{:T(128)} %constant.73.clone.1..sunk, s32[]{:T(128)} %constant.73.clone.1..sunk, s32[]{:T(128)} %constant.73.clone.1..sunk) | dynamic-update-slice | bytes 524292 | tf_op jit(solution)/shard_map/while/body/jit(dynamic_update_index_in_dim)/dynamic_update_slice | solution.py:118
  114.0 7.1 %dynamic_update_slice.28 = f32[2,128,8,64]{1,0,3,2:T(2,128)} dynamic-update-slice(f32[2,128,8,64]{1,0,3,2:T(2,128)} %get-tuple-element.314, f32[1,128,8,64]{1,0,3,2:T(1,128)S(1)} %bitcast.261, s32[]{:T(128)S(6)} %copy.169, s32[]{:T(128)} %constant.73.clone.1..sunk, s32[]{:T(128)} %constant.73.clone.1..sunk, s32[]{:T(128)} %constant.73.clone.1..sunk) | dynamic-update-slice | bytes 524292 | tf_op jit(solution)/shard_map/while/body/jit(dynamic_update_index_in_dim)/dynamic_update_slice | solution.py:118
  121.2 3.3 %stack_reshape.13 = f32[1,16,16384]{2,1,0:T(8,128)} reshape(f32[2,8,32,8,64]{4,3,2,1,0:T(8,128)} %get-tuple-element.82) | data formatting | bytes 2097152 | tf_op jit(solution)/shard_map/stack;reshape | solution.py:125
  124.5 1.6 stack_reshape.12
  126.1 3.1 %convolution_bitcast_fusion.2 = f32[2,24,16384]{2,1,0:T(8,128)S(1)} fusion(f32[1,16,16384]{2,1,0:T(8,128)} %stack_reshape.13, f32[1,16,16384]{2,1,0:T(8,128)} %stack_reshape.12, s32[16]{0:T(128)S(1)} %eq.46, pred[16]{0:T(512)(128)(4,1)S(1)} %and.45), kind=kOutput, calls=%fused_computation.80 | convolution fusion | flops 151520000 | bytes 5242960 | tf_op jit(solution)/shard_map/ab,xac->xbc/dot_general | solution.py:128
  130.3 1.6 copy.133
  131.9 4.3 %all-to-all-start.4 = ((f32[16,1,32,512]{3,2,1,0:T(8,128)}), f32[16,1,32,512]{3,2,1,0:T(8,128)}, u32[]{:S(2)}, u32[]{:S(2)}) async-start(f32[16,1,32,512]{3,2,1,0:T(8,128)} %bitcast.264), calls=%async_computation.4 | async-start | bytes 2097152 | tf_op jit(solution)/shard_map/all_to_all | solution.py:135
  136.3 2.8 copy.132
  139.1 20.0 %all-to-all-done.4 = f32[16,1,32,512]{3,2,1,0:T(8,128)} async-done(((f32[16,1,32,512]{3,2,1,0:T(8,128)}), f32[16,1,32,512]{3,2,1,0:T(8,128)}, u32[]{:S(2)}, u32[]{:S(2)}) %all-to-all-start.4) | async-done | bytes 1048608 | tf_op jit(solution)/shard_map/all_to_all | solution.py:135
  159.1 6.1 %all-to-all-start.3 = ((f32[16,1,32,512]{3,2,1,0:T(8,128)}), f32[16,1,32,512]{3,2,1,0:T(8,128)}, u32[]{:S(2)}, u32[]{:S(2)}) async-start(f32[16,1,32,512]{3,2,1,0:T(8,128)} %bitcast.263), calls=%async_computation.3 | async-start | bytes 2097152 | tf_op jit(solution)/shard_map/all_to_all | solution.py:134
  166.0 2.4 stack_reshape.15
  168.4 19.8 %all-to-all-done.3 = f32[16,1,32,512]{3,2,1,0:T(8,128)} async-done(((f32[16,1,32,512]{3,2,1,0:T(8,128)}), f32[16,1,32,512]{3,2,1,0:T(8,128)}, u32[]{:S(2)}, u32[]{:S(2)}) %all-to-all-start.3) | async-done | bytes 1048608 | tf_op jit(solution)/shard_map/all_to_all | solution.py:134
  188.1 2.4 stack_reshape.14
  190.5 2.3 fusion.59
  194.0 3.9 %convolution_bitcast_fusion.4 = f32[2048,512]{0,1:T(8,128)} fusion(bf16[256,512]{0,1:T(8,128)(2,1)S(1)} %fusion.66, bf16[256,2048]{1,0:T(8,128)(2,1)} %all-gather.2.cloned.1.call-done), kind=kOutput, calls=%fused_computation.83 | convolution fusion | flops 536870912 | bytes 5505024 | tf_op jit(solution)/shard_map/dot_general | solution.py:157
  202.4 91.4 %reduce-scatter.2.cloned.1.call-done = f32[128,512]{0,1:T(8,128)} async-done(((f32[2048,512]{0,1:T(8,128)}), f32[128,512]{0,1:T(8,128)}) %reduce-scatter.2.cloned.1.call-update) | async-done | bytes 262160 | tf_op jit(solution)/shard_map/reduce_scatter | solution.py:156
  293.8 1.8 copy.109
  (121 shorter events, 39.0 us)
Async XLA Ops:
  27.6 21.7 %copy-start.1 = (bf16[256,512]{1,0:T(8,128)(2,1)S(1)}, bf16[256,512]{1,0:T(8,128)(2,1)}, u32[]{:S(2)}) copy-start(bf16[256,512]{1,0:T(8,128)(2,1)} %param.11) | copy-start | bytes 786436
  27.6 22.8 %copy-start = (bf16[256,512]{1,0:T(8,128)(2,1)S(1)}, bf16[256,512]{1,0:T(8,128)(2,1)}, u32[]{:S(2)}) copy-start(bf16[256,512]{1,0:T(8,128)(2,1)} %param.10) | copy-start | bytes 786436
  28.6 22.3 %copy-start.9 = (bf16[256,512]{1,0:T(8,128)(2,1)S(1)}, bf16[256,512]{1,0:T(8,128)(2,1)}, u32[]{:S(2)}) copy-start(bf16[256,512]{1,0:T(8,128)(2,1)} %param.9) | copy-start | bytes 786436
  45.3 7.9 %copy-start.10 = (bf16[256,512]{1,0:T(8,128)(2,1)S(1)}, bf16[256,512]{1,0:T(8,128)(2,1)}, u32[]{:S(2)}) copy-start(bf16[256,512]{1,0:T(8,128)(2,1)} %param.13) | copy-start | bytes 786436
  45.3 18.0 %all-to-all-start.2 = ((bf16[16,1,32,512]{3,2,1,0:T(8,128)(2,1)}), bf16[16,1,32,512]{3,2,1,0:T(8,128)(2,1)S(1)}, u32[]{:S(2)}, u32[]{:S(2)}) async-start(bf16[16,1,32,512]{3,2,1,0:T(8,128)(2,1)} %get-tuple-element.202), calls=%async_computation.2 | async-start | bytes 1048576 | tf_op jit(solution)/shard_map/all_to_all | solution.py:98
  63.3 1.2 copy-start.11
  72.2 1.6 copy-start.5
  72.5 2.0 copy-start.2
  76.4 1.3 copy-start.3
  76.4 1.9 copy-start.6
  100.5 1.6 copy-start.5
  100.8 2.0 copy-start.2
  104.7 1.3 copy-start.3
  104.7 1.9 copy-start.6
  121.2 3.3 %copy-start.4 = (f32[2,8,32,8,64]{4,3,2,1,0:T(8,128)S(1)}, f32[2,8,32,8,64]{4,3,2,1,0:T(8,128)}, u32[]{:S(2)}) copy-start(f32[2,8,32,8,64]{4,3,2,1,0:T(8,128)} %get-tuple-element.81) | copy-start | bytes 3145732
  131.9 27.1 %all-to-all-start.4 = ((f32[16,1,32,512]{3,2,1,0:T(8,128)}), f32[16,1,32,512]{3,2,1,0:T(8,128)}, u32[]{:S(2)}, u32[]{:S(2)}) async-start(f32[16,1,32,512]{3,2,1,0:T(8,128)} %bitcast.264), calls=%async_computation.4 | async-start | bytes 2097152 | tf_op jit(solution)/shard_map/all_to_all | solution.py:135
  159.1 29.1 %all-to-all-start.3 = ((f32[16,1,32,512]{3,2,1,0:T(8,128)}), f32[16,1,32,512]{3,2,1,0:T(8,128)}, u32[]{:S(2)}, u32[]{:S(2)}) async-start(f32[16,1,32,512]{3,2,1,0:T(8,128)} %bitcast.263), calls=%async_computation.3 | async-start | bytes 2097152 | tf_op jit(solution)/shard_map/all_to_all | solution.py:134
  165.2 28.9 %all-gather.2.cloned.1.call-start = ((), (), s32[]{:S(2)}) async-start(), calls=%async_computation.6 | async-start | bytes 1572864 | tf_op jit(solution)/shard_map/all_gather | solution.py:155
  165.9 127.9 %reduce-scatter.2.cloned.1.call-start = ((), (), s32[]{:S(2)}) async-start(), calls=%async_computation.7 | async-start | bytes 4456448 | tf_op jit(solution)/shard_map/reduce_scatter | solution.py:156
  192.9 1.0 copy-start.8
  197.9 3.5 %copy-start.7 = (f32[2,128,8,64]{1,0,3,2:T(2,128)S(1)}, f32[2,128,8,64]{1,0,3,2:T(2,128)}, u32[]{:S(2)}) copy-start(f32[2,128,8,64]{1,0,3,2:T(2,128)} %get-tuple-element.83) | copy-start | bytes 1572868
Sparse Core Ops, SparseCore 0:
  167.5 10.2 all-gather.1
  198.1 95.6 reduce-scatter.1
where the time goes:
time: 305 us; the launch traced here: 302 us
  waiting for transfers between devices  135 us (44%)
  local copies, waits for them, and re-layouts  76.8 us (25%)
  blocking collectives  32.2 us (11%)
  matrix products  24.7 us (8%)
  starting transfers between devices  14.5 us (5%)
  between operations  14.3 us (5%)
  other arithmetic  4.52 us (1%)
    reduce_scatter x1, waiting for transfers between devices, body(): lax.psum_scatter(lax.dot_general(features_all, value_grad, (((0,), (0,)),...  91.4 us
    dynamic_update_slice x6, local copies, waits for them, and re-layouts, body(): lax.map(partial(block_grads, scaling=head_size ** (-0.5)), inputs)  32.3 us
    all_to_all x1, waiting for transfers between devices, body(): lax.all_to_all(back_values, 'kv', split_axis=0, concat_axis=0, tiled=True)  20 us
    all_to_all x1, waiting for transfers between devices, body(): lax.all_to_all(back_keys, 'kv', split_axis=0, concat_axis=0, tiled=True)  19.8 us
    all_to_all x1, blocking collectives, body(): lax.all_to_all(outgoing_keys, 'kv', split_axis=0, concat_axis=0, tiled=True)  16.8 us
    all_to_all x1, blocking collectives, body(): lax.all_to_all(wanted.reshape(devices, groups), 'kv', split_axis=0, conca...  15.4 us
    unnamed x23, local copies, waits for them, and re-layouts  10.9 us
    while x16, local copies, waits for them, and re-layouts  6.63 us
  transfers between devices with their start and end apart: 5, of which 4 were waited for; matrix products, arithmetic and copies ran while one was open for 8% of the time, Pallas kernels for 0%

commit v1 on v0

--- a/solution.py
+++ b/solution.py
@@ -6,6 +6,28 @@
 
 QB = 128
 KB = 32
+
+
+def in_blocks(x, dim, size):
+    before, after = (x.shape[:dim], x.shape[dim + 1 :])
+    return jnp.moveaxis(x.reshape(*before, size, -1, *after), dim, 0)
+
+
+def joined_along(pieces, dim):
+    lengths = list(pieces.shape[1:])
+    lengths[dim] *= pieces.shape[0]
+    return jnp.moveaxis(pieces, 0, dim).reshape(lengths)
+
+
+def swapped_with_each(x, axis, split_dim, concat_dim):
+    size, index = (lax.axis_size(axis), lax.axis_index(axis))
+    blocks = in_blocks(x, split_dim, size)
+    finished = [blocks[index]]
+    for lap in range(1, size):
+        sent = blocks[index ^ lap]
+        finished.append(lax.ppermute(sent, axis, [(i, i ^ lap) for i in range(size)]))
+    blocks = jnp.stack(finished)[index ^ jnp.arange(size)]
+    return joined_along(blocks, concat_dim)
 
 
 def block_grads(inputs, scaling):
@@ -131,7 +153,7 @@
     back_keys = routed[0, :slot_count].reshape(devices, groups, KB, columns)
     back_values = routed[1, :slot_count].reshape(devices, groups, KB, columns)
     returned_keys, returned_values = (
-        lax.all_to_all(back_keys, "kv", split_axis=0, concat_axis=0, tiled=True),
+        swapped_with_each(back_keys, "kv", 0, 0),
         lax.all_to_all(back_values, "kv", split_axis=0, concat_axis=0, tiled=True),
     )
     matched = (

time: 305 us -> 306 us (level)
  waiting for transfers between devices: 135 us -> 101 us
  starting transfers between devices: 14.5 us -> 38.9 us
  local copies, waits for them, and re-layouts: 76.8 us -> 87.4 us
    ppermute x0 -> x15, starting transfers between devices: none -> 30 us  [swapped_with_each(): lax.ppermute(sent, axis, [(i, i ^ lap) for i in range(size)])]
    all_to_all x1, waiting for transfers between devices: 20 us -> 0.01 us  [body(): lax.all_to_all(back_values, 'kv', split_axis=0, concat_axis=0, tiled=True)]
    all_to_all x1 -> x0, waiting for transfers between devices: 19.8 us -> none  [body(): lax.all_to_all(back_keys, 'kv', split_axis=0, concat_axis=0, tiled=True)]
    ppermute x0 -> x15, waiting for transfers between devices: none -> 7.91 us  [swapped_with_each(): lax.ppermute(sent, axis, [(i, i ^ lap) for i in range(size)])]
    unnamed x23 -> x37, local copies, waits for them, and re-layouts: 10.9 us -> 18.2 us
    all_to_all x1 -> x0, starting transfers between devices: 6.09 us -> none  [body(): lax.all_to_all(back_keys, 'kv', split_axis=0, concat_axis=0, tiled=True)]
  transfers between devices with their start and end apart: 5 -> 19, of which waited for: 4 -> 6; matrix products, arithmetic and copies ran while one was open for 8% -> 32% of each run, Pallas kernels for 0% -> 0%
where the time goes in v1:
time: 306 us; the launch traced here: 303 us
  waiting for transfers between devices  101 us (33%)
  local copies, waits for them, and re-layouts  87.4 us (29%)
  starting transfers between devices  38.9 us (13%)
  blocking collectives  32.2 us (11%)
  matrix products  24.7 us (8%)
  between operations  14.4 us (5%)
  other arithmetic  4.54 us (1%)
    reduce_scatter x1, waiting for transfers between devices, body(): lax.psum_scatter(lax.dot_general(features_all, value_grad, (((0,), (0,)),...  89.7 us
    dynamic_update_slice x6, local copies, waits for them, and re-layouts, body(): lax.map(partial(block_grads, scaling=head_size ** (-0.5)), inputs)  32.3 us
    ppermute x15, starting transfers between devices, swapped_with_each(): lax.ppermute(sent, axis, [(i, i ^ lap) for i in range(size)])  30 us
    unnamed x37, local copies, waits for them, and re-layouts  18.2 us
    all_to_all x1, blocking collectives, body(): lax.all_to_all(outgoing_keys, 'kv', split_axis=0, concat_axis=0, tiled=True)  16.8 us
    all_to_all x1, blocking collectives, body(): lax.all_to_all(wanted.reshape(devices, groups), 'kv', split_axis=0, conca...  15.4 us
    ppermute x15, waiting for transfers between devices, swapped_with_each(): lax.ppermute(sent, axis, [(i, i ^ lap) for i in range(size)])  7.91 us
    while x16, local copies, waits for them, and re-layouts  6.63 us
  transfers between devices with their start and end apart: 19, of which 6 were waited for; matrix products, arithmetic and copies ran while one was open for 32% of the time, Pallas kernels for 0%

profile of v1, /device:TPU:0, one launch (start us, length us, event | category | flops | bytes accessed | tf_op | source)
XLA Modules:
  0.0 303.5 jit_solution(5361922891811265612)
XLA Ops:
  8.1 15.4 %all_to_all.24 = s32[16,1,1]{2,1,0:T(1,128)S(1)} all-to-all(s32[16,1,1]{2,1,0:T(1,128)S(1)} %copy.84), channel_id=1, replica_groups=mesh['kv'=16,'tp'=2] {'kv'}, dimensions={0} | all-to-all | bytes 128 | tf_op jit(solution)/shard_map/all_to_all | solution.py:104
  28.6 16.8 %all_to_all.25 = bf16[16,1,32,512]{3,2,1,0:T(8,128)(2,1)S(1)} all-to-all(bf16[16,1,32,512]{3,2,1,0:T(8,128)(2,1)S(1)} %get-tuple-element.219), channel_id=1, replica_groups=mesh['kv'=16,'tp'=2] {'kv'}, dimensions={0} | all-to-all | bytes 1048576 | tf_op jit(solution)/shard_map/all_to_all | solution.py:119
  45.3 3.8 %all-to-all-start.2 = ((bf16[16,1,32,512]{3,2,1,0:T(8,128)(2,1)}), bf16[16,1,32,512]{3,2,1,0:T(8,128)(2,1)S(1)}, u32[]{:S(2)}, u32[]{:S(2)}) async-start(bf16[16,1,32,512]{3,2,1,0:T(8,128)(2,1)} %get-tuple-element.218), calls=%async_computation.2 | async-start | bytes 1048576 | tf_op jit(solution)/shard_map/all_to_all | solution.py:120
  56.3 2.0 copy.93
  60.7 2.5 all-to-all-done.2
  64.4 56.8 %while.18 = (s32[]{:T(128)}, bf16[2,128,8,64]{1,3,2,0:T(8,128)(2,1)}, f32[2,8,32,8,64]{4,3,2,1,0:T(8,128)}, f32[2,8,32,8,64]{4,3,2,1,0:T(8,128)}, f32[2,128,8,64...) while((s32[]{:T(128)}, ...), condition=%wide.region_3.4_spmd, body=%wide.region_1.3_spmd.sunk | while | flops 306330624 | bytes 43585888 | solution.py:140
  70.4 1.9 fusion.161
  74.6 1.9 copy_dynamic-update-slice_fusion.3
  78.4 7.1 %dynamic_update_slice.27 = f32[2,128,8,64]{1,0,3,2:T(2,128)} dynamic-update-slice(f32[2,128,8,64]{1,0,3,2:T(2,128)} %get-tuple-element.329, f32[1,128,8,64]{1,0,3,2:T(1,128)S(1)} %bitcast.321, s32[]{:T(128)S(6)} %copy.166, s32[]{:T(128)} %constant.42.clone.1..sunk, s32[]{:T(128)} %constant.42.clone.1..sunk, s32[]{:T(128)} %constant.42.clone.1..sunk) | dynamic-update-slice | bytes 524292 | tf_op jit(solution)/shard_map/while/body/jit(dynamic_update_index_in_dim)/dynamic_update_slice | solution.py:140
  85.8 7.1 %dynamic_update_slice.28 = f32[2,128,8,64]{1,0,3,2:T(2,128)} dynamic-update-slice(f32[2,128,8,64]{1,0,3,2:T(2,128)} %get-tuple-element.330, f32[1,128,8,64]{1,0,3,2:T(1,128)S(1)} %bitcast.320, s32[]{:T(128)S(6)} %copy.166, s32[]{:T(128)} %constant.42.clone.1..sunk, s32[]{:T(128)} %constant.42.clone.1..sunk, s32[]{:T(128)} %constant.42.clone.1..sunk) | dynamic-update-slice | bytes 524292 | tf_op jit(solution)/shard_map/while/body/jit(dynamic_update_index_in_dim)/dynamic_update_slice | solution.py:140
  98.8 1.9 fusion.161
  102.9 1.9 copy_dynamic-update-slice_fusion.3
  106.7 7.1 %dynamic_update_slice.27 = f32[2,128,8,64]{1,0,3,2:T(2,128)} dynamic-update-slice(f32[2,128,8,64]{1,0,3,2:T(2,128)} %get-tuple-element.329, f32[1,128,8,64]{1,0,3,2:T(1,128)S(1)} %bitcast.321, s32[]{:T(128)S(6)} %copy.166, s32[]{:T(128)} %constant.42.clone.1..sunk, s32[]{:T(128)} %constant.42.clone.1..sunk, s32[]{:T(128)} %constant.42.clone.1..sunk) | dynamic-update-slice | bytes 524292 | tf_op jit(solution)/shard_map/while/body/jit(dynamic_update_index_in_dim)/dynamic_update_slice | solution.py:140
  114.1 7.1 %dynamic_update_slice.28 = f32[2,128,8,64]{1,0,3,2:T(2,128)} dynamic-update-slice(f32[2,128,8,64]{1,0,3,2:T(2,128)} %get-tuple-element.330, f32[1,128,8,64]{1,0,3,2:T(1,128)S(1)} %bitcast.320, s32[]{:T(128)S(6)} %copy.166, s32[]{:T(128)} %constant.42.clone.1..sunk, s32[]{:T(128)} %constant.42.clone.1..sunk, s32[]{:T(128)} %constant.42.clone.1..sunk) | dynamic-update-slice | bytes 524292 | tf_op jit(solution)/shard_map/while/body/jit(dynamic_update_index_in_dim)/dynamic_update_slice | solution.py:140
  121.2 3.4 %stack_reshape.10 = f32[1,16,16384]{2,1,0:T(8,128)} reshape(f32[2,8,32,8,64]{4,3,2,1,0:T(8,128)} %get-tuple-element.82) | data formatting | bytes 2097152 | tf_op jit(solution)/shard_map/stack;reshape | solution.py:147
  126.2 3.1 %convolution_bitcast_fusion.2 = f32[2,24,16384]{2,1,0:T(8,128)S(1)} fusion(f32[1,16,16384]{2,1,0:T(8,128)} %stack_reshape.10, f32[1,16,16384]{2,1,0:T(8,128)} %stack_reshape.9, s32[16]{0:T(128)S(1)} %eq.46, pred[16]{0:T(512)(128)(4,1)S(1)} %and.45), kind=kOutput, calls=%fused_computation.81 | convolution fusion | flops 151520000 | bytes 5242960 | tf_op jit(solution)/shard_map/ab,xac->xbc/dot_general | solution.py:150
  133.1 4.8 %all-to-all-start.3 = ((f32[16,1,32,512]{3,2,1,0:T(8,128)}), f32[16,1,32,512]{3,2,1,0:T(8,128)}, u32[]{:S(2)}, u32[]{:S(2)}) async-start(f32[16,1,32,512]{3,2,1,0:T(8,128)} %bitcast.322), calls=%async_computation.3 | async-start | bytes 2097152 | tf_op jit(solution)/shard_map/all_to_all | solution.py:157
  138.2 1.9 collective-permute-start.1
  143.2 2.8 collective-permute-start.5
  150.0 3.6 %collective-permute-start.7 = (f32[1,1,32,512]{3,2,1,0:T(8,128)}, f32[1,1,32,512]{3,2,1,0:T(8,128)S(1)}, u32[]{:S(2)}, u32[]{:S(2)}) collective-permute-start(f32[1,1,32,512]{3,2,1,0:T(8,128)} %get-tuple-element.208), channel_id=1, source_target_pairs={{0,16},{2,18},{4,20},{6,22},{8,24},{10,26},{12,28},{14,30},{16,0},... | collective-permute-start | bytes 196616 | tf_op jit(solution)/shard_map/ppermute | solution.py:28
  154.2 3.2 %collective-permute-done.3 = f32[1,1,32,512]{3,2,1,0:T(8,128)S(1)} collective-permute-done((f32[1,1,32,512]{3,2,1,0:T(8,128)}, f32[1,1,32,512]{3,2,1,0:T(8,128)S(1)}, u32[]{:S(2)}, u32[]{:S(2)}) %collective-permute-start.3) | collective-permute-done | bytes 65568 | tf_op jit(solution)/shard_map/ppermute | solution.py:28
  157.4 5.7 %collective-permute-start.8 = (f32[1,1,32,512]{3,2,1,0:T(8,128)}, f32[1,1,32,512]{3,2,1,0:T(8,128)S(1)}, u32[]{:S(2)}, u32[]{:S(2)}) collective-permute-start(f32[1,1,32,512]{3,2,1,0:T(8,128)} %get-tuple-element.207), channel_id=1, source_target_pairs={{0,18},{2,16},{4,22},{6,20},{8,26},{10,24},{12,30},{14,28},{16,2},... | collective-permute-start | bytes 196616 | tf_op jit(solution)/shard_map/ppermute | solution.py:28
  166.1 2.2 collective-permute-start.10
  169.5 2.0 collective-permute-done.7
  171.5 2.6 collective-permute-start.12
  177.2 3.1 %collective-permute-start.14 = (f32[1,1,32,512]{3,2,1,0:T(8,128)S(1)}, f32[1,1,32,512]{3,2,1,0:T(8,128)S(1)}, u32[]{:S(2)}, u32[]{:S(2)}) collective-permute-start(f32[1,1,32,512]{3,2,1,0:T(8,128)S(1)} %get-tuple-element.201), channel_id=1, source_target_pairs={{0,30},{2,28},{4,26},{6,24},{8,22},{10,20},{12,18},{14,16},{16,14}... | collective-permute-start | bytes 196616 | tf_op jit(solution)/shard_map/ppermute | solution.py:28
  185.7 2.8 gather_fusion.4
  188.5 2.4 stack_reshape_reshape.3
  191.0 2.4 stack_reshape.11
  193.3 2.3 fusion.59
  196.8 3.9 %convolution_bitcast_fusion.4 = f32[2048,512]{0,1:T(8,128)} fusion(bf16[256,512]{0,1:T(8,128)(2,1)S(1)} %fusion.66, bf16[256,2048]{1,0:T(8,128)(2,1)} %all-gather.2.cloned.1.call-done), kind=kOutput, calls=%fused_computation.84 | convolution fusion | flops 536870912 | bytes 5505024 | tf_op jit(solution)/shard_map/dot_general | solution.py:179
  205.2 89.7 %reduce-scatter.2.cloned.1.call-done = f32[128,512]{0,1:T(8,128)} async-done(((f32[2048,512]{0,1:T(8,128)}), f32[128,512]{0,1:T(8,128)}) %reduce-scatter.2.cloned.1.call-update) | async-done | bytes 262160 | tf_op jit(solution)/shard_map/reduce_scatter | solution.py:178
  (168 shorter events, 70.3 us)
Async XLA Ops:
  27.6 22.3 %copy-start.1 = (bf16[256,512]{1,0:T(8,128)(2,1)S(1)}, bf16[256,512]{1,0:T(8,128)(2,1)}, u32[]{:S(2)}) copy-start(bf16[256,512]{1,0:T(8,128)(2,1)} %param.11) | copy-start | bytes 786436
  28.6 22.5 %copy-start = (bf16[256,512]{1,0:T(8,128)(2,1)S(1)}, bf16[256,512]{1,0:T(8,128)(2,1)}, u32[]{:S(2)}) copy-start(bf16[256,512]{1,0:T(8,128)(2,1)} %param.10) | copy-start | bytes 786436
  28.6 22.9 %copy-start.9 = (bf16[256,512]{1,0:T(8,128)(2,1)S(1)}, bf16[256,512]{1,0:T(8,128)(2,1)}, u32[]{:S(2)}) copy-start(bf16[256,512]{1,0:T(8,128)(2,1)} %param.9) | copy-start | bytes 786436
  45.3 17.8 %all-to-all-start.2 = ((bf16[16,1,32,512]{3,2,1,0:T(8,128)(2,1)}), bf16[16,1,32,512]{3,2,1,0:T(8,128)(2,1)S(1)}, u32[]{:S(2)}, u32[]{:S(2)}) async-start(bf16[16,1,32,512]{3,2,1,0:T(8,128)(2,1)} %get-tuple-element.218), calls=%async_computation.2 | async-start | bytes 1048576 | tf_op jit(solution)/shard_map/all_to_all | solution.py:120
  49.2 4.7 %copy-start.10 = (bf16[256,512]{1,0:T(8,128)(2,1)S(1)}, bf16[256,512]{1,0:T(8,128)(2,1)}, u32[]{:S(2)}) copy-start(bf16[256,512]{1,0:T(8,128)(2,1)} %param.13) | copy-start | bytes 786436
  49.2 147.6 %all-gather.2.cloned.1.call-start = ((), (), s32[]{:S(2)}) async-start(), calls=%async_computation.5 | async-start | bytes 1572864 | tf_op jit(solution)/shard_map/all_gather | solution.py:177
  72.3 1.6 copy-start.5
  72.6 2.0 copy-start.2
  76.5 1.9 copy-start.6
  100.6 1.6 copy-start.5
  100.9 2.0 copy-start.2
  104.8 1.3 copy-start.3
  104.8 1.9 copy-start.6
  121.2 3.4 %copy-start.4 = (f32[2,8,32,8,64]{4,3,2,1,0:T(8,128)S(1)}, f32[2,8,32,8,64]{4,3,2,1,0:T(8,128)}, u32[]{:S(2)}) copy-start(f32[2,8,32,8,64]{4,3,2,1,0:T(8,128)} %get-tuple-element.81) | copy-start | bytes 3145732
  131.0 12.2 %collective-permute-start = (f32[1,1,32,512]{3,2,1,0:T(8,128)}, f32[1,1,32,512]{3,2,1,0:T(8,128)}, u32[]{:S(2)}, u32[]{:S(2)}) collective-permute-start(f32[1,1,32,512]{3,2,1,0:T(8,128)} %get-tuple-element.215), channel_id=1, source_target_pairs={{0,2},{2,0},{4,6},{6,4},{8,10},{10,8},{12,14},{14,12},{16,18},{18,... | collective-permute-start | bytes 196616 | tf_op jit(solution)/shard_map/ppermute | solution.py:28
  133.1 57.9 %all-to-all-start.3 = ((f32[16,1,32,512]{3,2,1,0:T(8,128)}), f32[16,1,32,512]{3,2,1,0:T(8,128)}, u32[]{:S(2)}, u32[]{:S(2)}) async-start(f32[16,1,32,512]{3,2,1,0:T(8,128)} %bitcast.322), calls=%async_computation.3 | async-start | bytes 2097152 | tf_op jit(solution)/shard_map/all_to_all | solution.py:157
  137.9 157.0 %reduce-scatter.2.cloned.1.call-start = ((), (), s32[]{:S(2)}) async-start(), calls=%async_computation.6 | async-start | bytes 4456448 | tf_op jit(solution)/shard_map/reduce_scatter | solution.py:178
  138.2 10.2 %collective-permute-start.1 = (f32[1,1,32,512]{3,2,1,0:T(8,128)}, f32[1,1,32,512]{3,2,1,0:T(8,128)S(1)}, u32[]{:S(2)}, u32[]{:S(2)}) collective-permute-start(f32[1,1,32,512]{3,2,1,0:T(8,128)} %get-tuple-element.214), channel_id=1, source_target_pairs={{0,4},{2,6},{4,0},{6,2},{8,12},{10,14},{12,8},{14,10},{16,20},{18,... | collective-permute-start | bytes 196616 | tf_op jit(solution)/shard_map/ppermute | solution.py:28
  140.1 9.9 %collective-permute-start.2 = (f32[1,1,32,512]{3,2,1,0:T(8,128)}, f32[1,1,32,512]{3,2,1,0:T(8,128)S(1)}, u32[]{:S(2)}, u32[]{:S(2)}) collective-permute-start(f32[1,1,32,512]{3,2,1,0:T(8,128)} %get-tuple-element.213), channel_id=1, source_target_pairs={{0,6},{2,4},{4,2},{6,0},{8,14},{10,12},{12,10},{14,8},{16,22},{18,... | collective-permute-start | bytes 196616 | tf_op jit(solution)/shard_map/ppermute | solution.py:28
  141.6 15.8 %collective-permute-start.3 = (f32[1,1,32,512]{3,2,1,0:T(8,128)}, f32[1,1,32,512]{3,2,1,0:T(8,128)S(1)}, u32[]{:S(2)}, u32[]{:S(2)}) collective-permute-start(f32[1,1,32,512]{3,2,1,0:T(8,128)} %get-tuple-element.212), channel_id=1, source_target_pairs={{0,8},{2,10},{4,12},{6,14},{8,0},{10,2},{12,4},{14,6},{16,24},{18,... | collective-permute-start | bytes 196616 | tf_op jit(solution)/shard_map/ppermute | solution.py:28
  143.0 20.7 %collective-permute-start.4 = (f32[1,1,32,512]{3,2,1,0:T(8,128)}, f32[1,1,32,512]{3,2,1,0:T(8,128)S(1)}, u32[]{:S(2)}, u32[]{:S(2)}) collective-permute-start(f32[1,1,32,512]{3,2,1,0:T(8,128)} %get-tuple-element.211), channel_id=1, source_target_pairs={{0,10},{2,8},{4,14},{6,12},{8,2},{10,0},{12,6},{14,4},{16,26},{18,... | collective-permute-start | bytes 196616 | tf_op jit(solution)/shard_map/ppermute | solution.py:28
  143.2 22.9 %collective-permute-start.5 = (f32[1,1,32,512]{3,2,1,0:T(8,128)}, f32[1,1,32,512]{3,2,1,0:T(8,128)S(1)}, u32[]{:S(2)}, u32[]{:S(2)}) collective-permute-start(f32[1,1,32,512]{3,2,1,0:T(8,128)} %get-tuple-element.210), channel_id=1, source_target_pairs={{0,12},{2,14},{4,8},{6,10},{8,4},{10,6},{12,0},{14,2},{16,28},{18,... | collective-permute-start | bytes 196616 | tf_op jit(solution)/shard_map/ppermute | solution.py:28
  148.4 20.5 %collective-permute-start.6 = (f32[1,1,32,512]{3,2,1,0:T(8,128)}, f32[1,1,32,512]{3,2,1,0:T(8,128)S(1)}, u32[]{:S(2)}, u32[]{:S(2)}) collective-permute-start(f32[1,1,32,512]{3,2,1,0:T(8,128)} %get-tuple-element.209), channel_id=1, source_target_pairs={{0,14},{2,12},{4,10},{6,8},{8,6},{10,4},{12,2},{14,0},{16,30},{18,... | collective-permute-start | bytes 196616 | tf_op jit(solution)/shard_map/ppermute | solution.py:28
  150.0 21.5 %collective-permute-start.7 = (f32[1,1,32,512]{3,2,1,0:T(8,128)}, f32[1,1,32,512]{3,2,1,0:T(8,128)S(1)}, u32[]{:S(2)}, u32[]{:S(2)}) collective-permute-start(f32[1,1,32,512]{3,2,1,0:T(8,128)} %get-tuple-element.208), channel_id=1, source_target_pairs={{0,16},{2,18},{4,20},{6,22},{8,24},{10,26},{12,28},{14,30},{16,0},... | collective-permute-start | bytes 196616 | tf_op jit(solution)/shard_map/ppermute | solution.py:28
  157.4 17.4 %collective-permute-start.8 = (f32[1,1,32,512]{3,2,1,0:T(8,128)}, f32[1,1,32,512]{3,2,1,0:T(8,128)S(1)}, u32[]{:S(2)}, u32[]{:S(2)}) collective-permute-start(f32[1,1,32,512]{3,2,1,0:T(8,128)} %get-tuple-element.207), channel_id=1, source_target_pairs={{0,18},{2,16},{4,22},{6,20},{8,26},{10,24},{12,30},{14,28},{16,2},... | collective-permute-start | bytes 196616 | tf_op jit(solution)/shard_map/ppermute | solution.py:28
  163.7 13.5 %collective-permute-start.9 = (f32[1,1,32,512]{3,2,1,0:T(8,128)S(1)}, f32[1,1,32,512]{3,2,1,0:T(8,128)S(1)}, u32[]{:S(2)}, u32[]{:S(2)}) collective-permute-start(f32[1,1,32,512]{3,2,1,0:T(8,128)S(1)} %get-tuple-element.206), channel_id=1, source_target_pairs={{0,20},{2,22},{4,16},{6,18},{8,28},{10,30},{12,24},{14,26},{16,4},... | collective-permute-start | bytes 196616 | tf_op jit(solution)/shard_map/ppermute | solution.py:28
  166.1 14.8 %collective-permute-start.10 = (f32[1,1,32,512]{3,2,1,0:T(8,128)S(1)}, f32[1,1,32,512]{3,2,1,0:T(8,128)S(1)}, u32[]{:S(2)}, u32[]{:S(2)}) collective-permute-start(f32[1,1,32,512]{3,2,1,0:T(8,128)S(1)} %get-tuple-element.205), channel_id=1, source_target_pairs={{0,22},{2,20},{4,18},{6,16},{8,30},{10,28},{12,26},{14,24},{16,6},... | collective-permute-start | bytes 196616 | tf_op jit(solution)/shard_map/ppermute | solution.py:28
  168.9 12.6 %collective-permute-start.11 = (f32[1,1,32,512]{3,2,1,0:T(8,128)S(1)}, f32[1,1,32,512]{3,2,1,0:T(8,128)S(1)}, u32[]{:S(2)}, u32[]{:S(2)}) collective-permute-start(f32[1,1,32,512]{3,2,1,0:T(8,128)S(1)} %get-tuple-element.204), channel_id=1, source_target_pairs={{0,24},{2,26},{4,28},{6,30},{8,16},{10,18},{12,20},{14,22},{16,8},... | collective-permute-start | bytes 196616 | tf_op jit(solution)/shard_map/ppermute | solution.py:28
  171.5 10.6 %collective-permute-start.12 = (f32[1,1,32,512]{3,2,1,0:T(8,128)S(1)}, f32[1,1,32,512]{3,2,1,0:T(8,128)S(1)}, u32[]{:S(2)}, u32[]{:S(2)}) collective-permute-start(f32[1,1,32,512]{3,2,1,0:T(8,128)S(1)} %get-tuple-element.203), channel_id=1, source_target_pairs={{0,26},{2,24},{4,30},{6,28},{8,18},{10,16},{12,22},{14,20},{16,10}... | collective-permute-start | bytes 196616 | tf_op jit(solution)/shard_map/ppermute | solution.py:28
  174.8 8.0 %collective-permute-start.13 = (f32[1,1,32,512]{3,2,1,0:T(8,128)S(1)}, f32[1,1,32,512]{3,2,1,0:T(8,128)S(1)}, u32[]{:S(2)}, u32[]{:S(2)}) collective-permute-start(f32[1,1,32,512]{3,2,1,0:T(8,128)S(1)} %get-tuple-element.202), channel_id=1, source_target_pairs={{0,28},{2,30},{4,24},{6,26},{8,20},{10,22},{12,16},{14,18},{16,12}... | collective-permute-start | bytes 196616 | tf_op jit(solution)/shard_map/ppermute | solution.py:28
  177.2 8.0 %collective-permute-start.14 = (f32[1,1,32,512]{3,2,1,0:T(8,128)S(1)}, f32[1,1,32,512]{3,2,1,0:T(8,128)S(1)}, u32[]{:S(2)}, u32[]{:S(2)}) collective-permute-start(f32[1,1,32,512]{3,2,1,0:T(8,128)S(1)} %get-tuple-element.201), channel_id=1, source_target_pairs={{0,30},{2,28},{4,26},{6,24},{8,22},{10,20},{12,18},{14,16},{16,14}... | collective-permute-start | bytes 196616 | tf_op jit(solution)/shard_map/ppermute | solution.py:28
  200.7 3.5 %copy-start.7 = (f32[2,128,8,64]{1,0,3,2:T(2,128)S(1)}, f32[2,128,8,64]{1,0,3,2:T(2,128)}, u32[]{:S(2)}) copy-start(f32[2,128,8,64]{1,0,3,2:T(2,128)} %get-tuple-element.83) | copy-start | bytes 1572868
  (3 other events, 3.6 us)
Sparse Core Ops, SparseCore 0:
  51.5 10.3 all-gather.1
  200.9 93.9 reduce-scatter.1
